TPU v7x, 32 devices: a whole 2x2x4 slice. The times are simulated.
32 devices in a mesh: grp: 2 (over y), sp: 4 (over z), tp: 4 (over x, core).
Axes of the slice: x: 2, y: 2, z: 4, core: 2. Of those that a mesh axis runs over, the one named last changes fastest.
Arguments:
- stream: bfloat16 [2048, 2048], P(('grp', 'sp')), parts along dimension 0, may hold values from -6 to 6
- doc_ids: int32 [2048], P(('grp', 'sp')), parts along dimension 0, may hold values from 0 to 1, never falling along the last dimension, each value on 1 to 768 neighbouring positions
- norm_gain: float32 [2, 2048], replicated, may hold values from 0.1 to 1.9
- query_weight: bfloat16 [2, 2048, 1024], P(None, 'sp', 'tp'), may hold values from -0.125 to 0.125
- key_weight: bfloat16 [2, 2048, 1024], P(None, 'sp', 'tp'), may hold values from -0.125 to 0.125
- value_weight: bfloat16 [2, 2048, 1024], P(None, 'sp', 'tp'), may hold values from -0.125 to 0.125
- out_weight: bfloat16 [2, 1024, 2048], P(None, 'sp', 'tp'), may hold values from -0.75 to 0.75
- query_gain: float32 [2, 64], replicated, may hold values from 0.1 to 1.9
- key_gain: float32 [2, 64], replicated, may hold values from 0.1 to 1.9
- rel_bias: float32 [16, 513], P('tp'), may hold values from -4 to 250
Outputs:
- encoded: bfloat16 [2048, 2048], P(('grp', 'sp')), parts along dimension 0
There are 2 independent parts, one for each index of `grp`. A program takes and returns all parts, laid end to end along the dimension named above; an argument that names none is the same for every part. Nothing has to cross between parts.
Inputs may be any that keep to these rules, and one draw needn't show every extreme that they name: doc_ids never fall along the sequence; each document has at most 768 positions.
All inputs are finite; a program needn't handle non-finite values.
Results may differ from a plain program's by a relative error of at most 0.011.
Values may be sent and summed in bfloat16 or wider, within the bound.
No kernel may reach another device: no remote copies, remote signals or barrier semaphores. Data moves between devices by JAX's collectives and lax.ppermute only.
A program may use at most 64 MiB of HBM per device.

v0:
```python
import jax
import jax.numpy as jnp
from jax import lax
from jax.sharding import PartitionSpec as P

SEG = 64
LEFT = 8
MAXREL = 256
LAYERS = 2
epsilon = 1e-06


def shifted(value, axis, steps):
    count = lax.axis_size(axis)
    initial, last = (max(0, -steps), min(count, count - steps))
    return lax.ppermute(value, axis, [(source, source + steps) for source in range(initial, last)])


def row_norm(values, gain):
    return values * lax.rsqrt(jnp.mean(values * values, axis=-1, keepdims=True) + epsilon) * gain


def bias_table(rel_bias):
    heads_here = rel_bias.shape[0]
    reach = LEFT * SEG
    width = (LEFT + 1) * SEG
    highest = reach + SEG - 1
    reversed_bias = rel_bias[:, ::-1]
    upper_fill = jnp.broadcast_to(rel_bias[:, -1:], (heads_here, highest - MAXREL))
    flat_row = jnp.concatenate([upper_fill, reversed_bias[:, : MAXREL + SEG]], axis=1)
    lines = [
        flat_row[:, SEG - 1 - position : SEG - 1 - position + width] for position in range(SEG)
    ]
    return jnp.stack(lines, axis=1)


def attend(query, ext_keys, ext_values, ext_docs, own_docs, offset, table):
    rows, heads_here, head_size = query.shape
    count = rows // SEG
    width = (LEFT + 1) * SEG
    blocks = query.reshape(count, SEG, heads_here, head_size)
    key_blocks = ext_keys.reshape(count + LEFT, SEG, heads_here, head_size)
    value_blocks = ext_values.reshape(count + LEFT, SEG, heads_here, head_size)
    doc_blocks = ext_docs.reshape(count + LEFT, SEG)
    score_parts = [
        jnp.einsum(
            "nqhd,nkhd->nhqk",
            blocks,
            key_blocks[earlier : earlier + count],
            preferred_element_type=jnp.float32,
        )
        for earlier in range(LEFT + 1)
    ]
    scores = jnp.concatenate(score_parts, axis=-1)
    scores = scores * head_size ** (-0.5) + table[None]
    doc_band = jnp.concatenate(
        [doc_blocks[earlier : earlier + count] for earlier in range(LEFT + 1)], axis=1
    )
    key_pos = (
        offset
        + SEG * jnp.arange(count, dtype=jnp.int32)[:, None]
        - LEFT * SEG
        + jnp.arange(width, dtype=jnp.int32)[None, :]
    )
    allowed = (key_pos >= 0)[:, None, None, :] & (
        doc_band[:, None, None, :] == own_docs.reshape(count, SEG)[:, None, :, None]
    )
    scores = jnp.where(allowed, scores, -1e30)
    peak = jnp.max(scores, axis=-1, keepdims=True)
    expo = jnp.exp(scores - peak)
    weights = (expo / jnp.sum(expo, axis=-1, keepdims=True)).astype(jnp.bfloat16)
    mixed = jnp.zeros((count, SEG, heads_here, head_size), jnp.float32)
    for earlier in range(LEFT + 1):
        part_weights = weights[..., earlier * SEG : (earlier + 1) * SEG]
        mixed = mixed + jnp.einsum(
            "nhqk,nkhd->nqhd",
            part_weights,
            value_blocks[earlier : earlier + count],
            preferred_element_type=jnp.float32,
        )
    return mixed.astype(jnp.bfloat16).reshape(rows, heads_here * head_size)


def on_device(
    stream,
    doc_ids,
    norm_gain,
    query_weight,
    key_weight,
    value_weight,
    out_weight,
    query_gain,
    key_gain,
    rel_bias,
):
    rows = stream.shape[0]
    heads_here = rel_bias.shape[0]
    head_size = query_gain.shape[1]
    local_width = heads_here * head_size
    reach = LEFT * SEG
    depth = -(-reach // rows)
    offset = lax.axis_index("sp") * rows
    col_width = out_weight.shape[2]
    col_start = lax.axis_index("tp") * col_width
    table = bias_table(rel_bias)
    x = stream
    for layer in range(LAYERS):
        widened = x.astype(jnp.float32)
        normed = row_norm(widened, norm_gain[layer]).astype(jnp.bfloat16)
        own_cols = normed
        q_raw = jnp.dot(
            own_cols,
            lax.all_gather(query_weight[layer], "sp", axis=0, tiled=True),
            preferred_element_type=jnp.float32,
        )
        k_raw = jnp.dot(
            normed,
            lax.all_gather(key_weight[layer], "sp", axis=0, tiled=True),
            preferred_element_type=jnp.float32,
        )
        v_raw = jnp.dot(
            normed,
            lax.all_gather(value_weight[layer], "sp", axis=0, tiled=True),
            preferred_element_type=jnp.float32,
        )
        query = row_norm(q_raw.reshape(rows, heads_here, head_size), query_gain[layer]).astype(
            jnp.bfloat16
        )
        keys = row_norm(
            k_raw.reshape(normed.shape[0], heads_here, head_size), key_gain[layer]
        ).astype(jnp.bfloat16)
        values = v_raw.astype(jnp.bfloat16)
        flat_keys = keys.reshape(rows, local_width)
        tail = (flat_keys, values, doc_ids)
        received = [
            shifted((tail[0], tail[1], tail[2]), "sp", distance_back)
            for distance_back in range(depth, 0, -1)
        ]
        ext_keys = jnp.concatenate([item[0] for item in received] + [flat_keys], axis=0)
        ext_values = jnp.concatenate([item[1] for item in received] + [values], axis=0)
        ext_docs = jnp.concatenate([item[2] for item in received] + [doc_ids], axis=0)
        ext_keys = ext_keys.reshape(reach + rows, heads_here, head_size)
        ext_values = ext_values.reshape(reach + rows, heads_here, head_size)
        attended = attend(query, ext_keys, ext_values, ext_docs, doc_ids, offset, table)
        all_heads = lax.all_gather(attended, "tp", axis=1, tiled=True)
        projected = jnp.dot(
            all_heads,
            lax.all_gather(out_weight[layer], "sp", axis=0, tiled=True),
            preferred_element_type=jnp.float32,
        )
        own_cols = lax.dynamic_slice_in_dim(widened, col_start, col_width, 1)
        new_cols = (own_cols + projected).astype(jnp.bfloat16)
        x = lax.all_gather(new_cols, "tp", axis=1, tiled=True)
    return x


def solution(mesh):
    placed = (
        P(("grp", "sp"), None),
        P(("grp", "sp")),
        P(),
        P(None, "sp", "tp"),
        P(None, "sp", "tp"),
        P(None, "sp", "tp"),
        P(None, "sp", "tp"),
        P(),
        P(),
        P("tp", None),
    )
    return jax.shard_map(
        on_device, mesh=mesh, in_specs=placed, out_specs=P(("grp", "sp"), None), check_vma=False
    )
```

profile of v0, /device:TPU:0, one launch (start us, length us, event | category | flops | bytes accessed | tf_op | source)
XLA Modules:
  0.0 338.0 jit_solution(15381538330978030332)
XLA Ops:
  6.5 2.0 fusion.257
  8.6 2.0 fusion.256
  11.6 6.0 %collective-permute-start.1 = (s32[256]{0:T(256)S(1)}, s32[256]{0:T(256)S(1)}, u32[]{:S(2)}, u32[]{:S(2)}) collective-permute-start(s32[256]{0:T(256)S(1)} %copy-done.17), channel_id=1, source_target_pairs={{0,8},{4,12},{1,9},{5,13},{2,10},{6,14},{3,11},{7,15},{16,24},{20,... | collective-permute-start | bytes 3080 | tf_op jit(solution)/shard_map/ppermute | solution.py:16
  17.5 3.5 %collective-permute-start.2 = (s32[256]{0:T(256)S(1)}, s32[256]{0:T(256)S(1)}, u32[]{:S(2)}, u32[]{:S(2)}) collective-permute-start(s32[256]{0:T(256)S(1)} %copy-done.17), channel_id=1, source_target_pairs={{0,4},{4,8},{8,12},{1,5},{5,9},{9,13},{2,6},{6,10},{10,14},{3,7},{... | collective-permute-start | bytes 3080 | tf_op jit(solution)/shard_map/ppermute | solution.py:16
  28.4 1.6 convert_element_type.52
  30.6 9.0 %all-gather.27.cloned.1.call-done = bf16[1,2048,256]{2,1,0:T(8,128)(2,1)} async-done(((bf16[1,512,256]{2,1,0:T(8,128)(2,1)}), bf16[1,2048,256]{2,1,0:T(8,128)(2,1)}) %all-gather.27.cloned.1.call-update) | async-done | bytes 1048592 | tf_op jit(solution)/shard_map/all_gather | solution.py:118
  39.7 1.9 bitcast_reduce_fusion.2
  41.7 3.7 %collective-permute-start.3 = (bf16[256,256]{0,1:T(8,128)(2,1)S(1)}, bf16[256,256]{0,1:T(8,128)(2,1)S(1)}, u32[]{:S(2)}, u32[]{:S(2)}) collective-permute-start(bf16[256,256]{0,1:T(8,128)(2,1)S(1)} %fusion.61), channel_id=1, source_target_pairs={{0,8},{4,12},{1,9},{5,13},{2,10},{6,14},{3,11},{7,15},{16,24},{20,... | collective-permute-start | bytes 393224 | tf_op jit(solution)/shard_map/ppermute | solution.py:16
  45.4 2.5 collective-permute-start.4
  48.0 20.7 %all-gather.23.cloned.1.call-done = bf16[1,2048,256]{2,1,0:T(8,128)(2,1)} async-done(((bf16[1,512,256]{2,1,0:T(8,128)(2,1)}), bf16[1,2048,256]{2,1,0:T(8,128)(2,1)}) %all-gather.23.cloned.1.call-update) | async-done | bytes 1048592 | tf_op jit(solution)/shard_map/all_gather | solution.py:123
  68.8 1.7 convolution_convert_fusion.1
  70.5 5.6 %collective-permute-start.5 = (bf16[256,256]{1,0:T(8,128)(2,1)S(1)}, bf16[256,256]{1,0:T(8,128)(2,1)S(1)}, u32[]{:S(2)}, u32[]{:S(2)}) collective-permute-start(bf16[256,256]{1,0:T(8,128)(2,1)S(1)} %convolution_convert_fusion.1), channel_id=1, source_target_pairs={{0,4},{4,8},{8,12},{1,5},{5,9},{9,13},{2,6},{6,10},{10,14},{3,7},{... | collective-permute-start | bytes 393224 | tf_op jit(solution)/shard_map/ppermute | solution.py:16
  76.1 4.3 %collective-permute-start = (bf16[256,256]{1,0:T(8,128)(2,1)S(1)}, bf16[256,256]{1,0:T(8,128)(2,1)S(1)}, u32[]{:S(2)}, u32[]{:S(2)}) collective-permute-start(bf16[256,256]{1,0:T(8,128)(2,1)S(1)} %convolution_convert_fusion.1), channel_id=1, source_target_pairs={{0,8},{4,12},{1,9},{5,13},{2,10},{6,14},{3,11},{7,15},{16,24},{20,... | collective-permute-start | bytes 393224 | tf_op jit(solution)/shard_map/ppermute | solution.py:16
  81.3 19.7 %all-gather.25.cloned.1.call-done = bf16[1,2048,256]{2,1,0:T(8,128)(2,1)} async-done(((bf16[1,512,256]{2,1,0:T(8,128)(2,1)}), bf16[1,2048,256]{2,1,0:T(8,128)(2,1)}) %all-gather.25.cloned.1.call-update) | async-done | bytes 1048592 | tf_op jit(solution)/shard_map/all_gather | solution.py:113
  101.0 1.9 bitcast_reduce_fusion.3
  118.7 3.6 %concatenate.92 = f32[4,4,64,576]{3,2,1,0:T(8,128)S(1)} concatenate(f32[4,4,64,64]{3,2,1,0:T(8,128)} %fusion.114, f32[4,4,64,64]{3,2,1,0:T(8,128)} %fusion.112, f32[4,4,64,64]{3,2,1,0:T(8,128)} %fusion.110, f32[4,4,64,64]{3,2,1,0:T(8,128)} %fusion.108, f32[4,4,64,64]{3,2,1,0:T(8,128)} %fusion.106, f32[4,4,64,64]{3,2,1,0:T(8,128)} %fusion.104, f32[4,4,64,64]{3,2,1,0:T(8,128)} %fusion.102, ...), dimensions={3} | concatenate | bytes 4718592 | tf_op jit(solution)/shard_map/concatenate | solution.py:54
  125.0 1.8 slice.569
  126.8 1.3 fusion.15
  128.0 1.3 fusion.49
  129.3 1.8 slice.670
  133.3 1.8 slice.672
  135.1 1.3 convolution_add_fusion.12
  136.4 1.3 fusion.14
  139.4 8.7 %all_gather.39 = bf16[256,1024]{1,0:T(8,128)(2,1)S(1)} all-gather(bf16[256,256]{1,0:T(8,128)(2,1)S(1)} %reshape.224), channel_id=1, replica_groups=mesh['grp'=2,'sp'=4,'tp'=4] {'tp'}, dimensions={1}, use_global_device_ids=true | all-gather | bytes 655360 | tf_op jit(solution)/shard_map/all_gather | solution.py:145
  148.1 2.5 fusion.16
  153.6 15.3 %all-gather.19.cloned.1.call-done = bf16[256,2048]{1,0:T(8,128)(2,1)} async-done(((bf16[256,512]{1,0:T(8,128)(2,1)}), bf16[256,2048]{1,0:T(8,128)(2,1)}) %all-gather.19.cloned.1.call-update) | async-done | bytes 1048592 | tf_op jit(solution)/shard_map/all_gather | solution.py:153
  168.9 1.5 multiply_reduce_fusion
  170.4 27.9 %all-gather.35.cloned.1.call-done = bf16[1,2048,256]{2,1,0:T(8,128)(2,1)} async-done(((bf16[1,512,256]{2,1,0:T(8,128)(2,1)}), bf16[1,2048,256]{2,1,0:T(8,128)(2,1)}) %all-gather.35.cloned.1.call-update) | async-done | bytes 1048592 | tf_op jit(solution)/shard_map/all_gather | solution.py:118
  198.3 2.2 bitcast_reduce_fusion
  200.6 3.7 %collective-permute-start.7 = (bf16[256,256]{0,1:T(8,128)(2,1)S(1)}, bf16[256,256]{0,1:T(8,128)(2,1)S(1)}, u32[]{:S(2)}, u32[]{:S(2)}) collective-permute-start(bf16[256,256]{0,1:T(8,128)(2,1)S(1)} %fusion.59), channel_id=1, source_target_pairs={{0,8},{4,12},{1,9},{5,13},{2,10},{6,14},{3,11},{7,15},{16,24},{20,... | collective-permute-start | bytes 393224 | tf_op jit(solution)/shard_map/ppermute | solution.py:16
  204.4 3.1 collective-permute-start.8
  207.7 19.0 %all-gather.31.cloned.1.call-done = bf16[1,2048,256]{2,1,0:T(8,128)(2,1)} async-done(((bf16[1,512,256]{2,1,0:T(8,128)(2,1)}), bf16[1,2048,256]{2,1,0:T(8,128)(2,1)}) %all-gather.31.cloned.1.call-update) | async-done | bytes 1048592 | tf_op jit(solution)/shard_map/all_gather | solution.py:123
  226.7 2.4 convolution_convert_fusion
  229.1 7.3 %collective-permute-start.9 = (bf16[256,256]{1,0:T(8,128)(2,1)}, bf16[256,256]{1,0:T(8,128)(2,1)}, u32[]{:S(2)}, u32[]{:S(2)}) collective-permute-start(bf16[256,256]{1,0:T(8,128)(2,1)} %convolution_convert_fusion), channel_id=1, source_target_pairs={{0,4},{4,8},{8,12},{1,5},{5,9},{9,13},{2,6},{6,10},{10,14},{3,7},{... | collective-permute-start | bytes 393224 | tf_op jit(solution)/shard_map/ppermute | solution.py:16
  236.4 4.2 %collective-permute-start.6 = (bf16[256,256]{1,0:T(8,128)(2,1)}, bf16[256,256]{1,0:T(8,128)(2,1)}, u32[]{:S(2)}, u32[]{:S(2)}) collective-permute-start(bf16[256,256]{1,0:T(8,128)(2,1)} %convolution_convert_fusion), channel_id=1, source_target_pairs={{0,8},{4,12},{1,9},{5,13},{2,10},{6,14},{3,11},{7,15},{16,24},{20,... | collective-permute-start | bytes 393224 | tf_op jit(solution)/shard_map/ppermute | solution.py:16
  240.6 1.8 slice.729
  242.4 18.9 %all-gather.33.cloned.1.call-done = bf16[1,2048,256]{2,1,0:T(8,128)(2,1)} async-done(((bf16[1,512,256]{2,1,0:T(8,128)(2,1)}), bf16[1,2048,256]{2,1,0:T(8,128)(2,1)}) %all-gather.33.cloned.1.call-update) | async-done | bytes 1048592 | tf_op jit(solution)/shard_map/all_gather | solution.py:113
  261.2 1.9 bitcast_reduce_fusion.1
  263.9 1.6 convert_element_type.60
  267.7 1.3 pad_maximum_fusion.1
  278.4 3.6 %concatenate.98 = f32[4,4,64,576]{3,2,1,0:T(8,128)S(1)} concatenate(f32[4,4,64,64]{3,2,1,0:T(8,128)} %fusion.87, f32[4,4,64,64]{3,2,1,0:T(8,128)} %fusion.85, f32[4,4,64,64]{3,2,1,0:T(8,128)} %fusion.83, f32[4,4,64,64]{3,2,1,0:T(8,128)} %fusion.81, f32[4,4,64,64]{3,2,1,0:T(8,128)} %fusion.79, f32[4,4,64,64]{3,2,1,0:T(8,128)} %fusion.77, f32[4,4,64,64]{3,2,1,0:T(8,128)} %fusion.75, ...), dimensions={3} | concatenate | bytes 4718592 | tf_op jit(solution)/shard_map/concatenate | solution.py:54
  282.0 2.3 fusion.267
  285.5 1.8 pad_maximum_fusion
  292.4 1.3 fusion.13
  299.8 8.3 %all_gather.45 = bf16[256,1024]{1,0:T(8,128)(2,1)S(1)} all-gather(bf16[256,256]{1,0:T(8,128)(2,1)S(1)} %reshape.226), channel_id=1, replica_groups=mesh['grp'=2,'sp'=4,'tp'=4] {'tp'}, dimensions={1}, use_global_device_ids=true | all-gather | bytes 655360 | tf_op jit(solution)/shard_map/all_gather | solution.py:145
  308.1 2.5 fusion.17
  310.7 18.2 %all-gather.21.cloned.1.call-done = bf16[256,2048]{1,0:T(8,128)(2,1)} async-done(((bf16[256,512]{1,0:T(8,128)(2,1)}), bf16[256,2048]{1,0:T(8,128)(2,1)}) %all-gather.21.cloned.1.call-update) | async-done | bytes 1048592 | tf_op jit(solution)/shard_map/all_gather | solution.py:153
  328.9 2.3 copy.233
  (259 shorter events, 59.8 us)
Async XLA Ops:
  6.5 4.1 %copy-start.12 = (bf16[2,512,256]{2,1,0:T(8,128)(2,1)S(1)}, bf16[2,512,256]{2,1,0:T(8,128)(2,1)}, u32[]{:S(2)}) copy-start(bf16[2,512,256]{2,1,0:T(8,128)(2,1)} %param.13) | copy-start | bytes 1572868
  6.5 5.0 %copy-start.17 = (s32[256]{0:T(256)S(1)}, s32[256]{0:T(256)}, u32[]{:S(2)}) copy-start(s32[256]{0:T(256)} %param.11) | copy-start | bytes 3076
  6.5 14.5 %copy-start.13 = (bf16[2,256,512]{2,1,0:T(8,128)(2,1)S(1)}, bf16[2,256,512]{2,1,0:T(8,128)(2,1)}, u32[]{:S(2)}) copy-start(bf16[2,256,512]{2,1,0:T(8,128)(2,1)} %param.16) | copy-start | bytes 1572868
  6.5 33.1 %all-gather.27.cloned.1.call-start = ((), (), s32[]{:S(2)}) async-start(), calls=%async_computation.4 | async-start | bytes 1310720 | tf_op jit(solution)/shard_map/all_gather | solution.py:118
  8.5 13.5 %copy-start.16 = (f32[4,513]{1,0:T(4,128)S(1)}, f32[4,513]{1,0:T(4,128)}, u32[]{:S(2)}) copy-start(f32[4,513]{1,0:T(4,128)} %param.19) | copy-start | bytes 24628
  8.5 13.7 %copy-start.15 = (f32[2,2048]{1,0:T(2,128)S(1)}, f32[2,2048]{1,0:T(2,128)}, u32[]{:S(2)}) copy-start(f32[2,2048]{1,0:T(2,128)} %param.12) | copy-start | bytes 49156
  8.5 13.7 %copy-start.3 = (bf16[256,2048]{1,0:T(8,128)(2,1)S(1)}, bf16[256,2048]{1,0:T(8,128)(2,1)}, u32[]{:S(2)}) copy-start(bf16[256,2048]{1,0:T(8,128)(2,1)} %param.10) | copy-start | bytes 3145732
  8.5 60.2 %all-gather.23.cloned.1.call-start = ((), (), s32[]{:S(2)}) async-start(), calls=%async_computation.2 | async-start | bytes 1310720 | tf_op jit(solution)/shard_map/all_gather | solution.py:123
  10.5 12.0 %copy-start.18 = (f32[2,64]{1,0:T(2,128)S(1)}, f32[2,64]{1,0:T(2,128)}, u32[]{:S(2)}) copy-start(f32[2,64]{1,0:T(2,128)} %param.17) | copy-start | bytes 1540
  10.5 12.0 %copy-start.19 = (f32[2,64]{1,0:T(2,128)S(1)}, f32[2,64]{1,0:T(2,128)}, u32[]{:S(2)}) copy-start(f32[2,64]{1,0:T(2,128)} %param.18) | copy-start | bytes 1540
  10.6 90.5 %all-gather.25.cloned.1.call-start = ((), (), s32[]{:S(2)}) async-start(), calls=%async_computation.3 | async-start | bytes 1310720 | tf_op jit(solution)/shard_map/all_gather | solution.py:113
  11.5 136.6 %all-gather.29.cloned.1.call-start = ((), (), s32[]{:S(2)}) async-start(), calls=%async_computation.5 | async-start | bytes 1310720 | tf_op jit(solution)/shard_map/all_gather | solution.py:148
  11.6 18.6 %collective-permute-start.1 = (s32[256]{0:T(256)S(1)}, s32[256]{0:T(256)S(1)}, u32[]{:S(2)}, u32[]{:S(2)}) collective-permute-start(s32[256]{0:T(256)S(1)} %copy-done.17), channel_id=1, source_target_pairs={{0,8},{4,12},{1,9},{5,13},{2,10},{6,14},{3,11},{7,15},{16,24},{20,... | collective-permute-start | bytes 3080 | tf_op jit(solution)/shard_map/ppermute | solution.py:16
  17.5 12.7 %collective-permute-start.2 = (s32[256]{0:T(256)S(1)}, s32[256]{0:T(256)S(1)}, u32[]{:S(2)}, u32[]{:S(2)}) collective-permute-start(s32[256]{0:T(256)S(1)} %copy-done.17), channel_id=1, source_target_pairs={{0,4},{4,8},{8,12},{1,5},{5,9},{9,13},{2,6},{6,10},{10,14},{3,7},{... | collective-permute-start | bytes 3080 | tf_op jit(solution)/shard_map/ppermute | solution.py:16
  21.9 147.0 %all-gather.19.cloned.1.call-start = ((), (), s32[]{:S(2)}) async-start(), calls=%async_computation | async-start | bytes 1310720 | tf_op jit(solution)/shard_map/all_gather | solution.py:153
  30.6 91.7 %copy-start.5 = (pred[4,64,576]{2,1,0:T(8,128)(4,1)}, pred[4,64,576]{2,1,0:T(8,128)(4,1)S(1)}, u32[]{:S(2)}) copy-start(pred[4,64,576]{2,1,0:T(8,128)(4,1)S(1)} %compare_and_fusion) | copy-start | bytes 442372
  41.7 63.0 %collective-permute-start.3 = (bf16[256,256]{0,1:T(8,128)(2,1)S(1)}, bf16[256,256]{0,1:T(8,128)(2,1)S(1)}, u32[]{:S(2)}, u32[]{:S(2)}) collective-permute-start(bf16[256,256]{0,1:T(8,128)(2,1)S(1)} %fusion.61), channel_id=1, source_target_pairs={{0,8},{4,12},{1,9},{5,13},{2,10},{6,14},{3,11},{7,15},{16,24},{20,... | collective-permute-start | bytes 393224 | tf_op jit(solution)/shard_map/ppermute | solution.py:16
  45.4 60.5 %collective-permute-start.4 = (bf16[256,256]{0,1:T(8,128)(2,1)S(1)}, bf16[256,256]{0,1:T(8,128)(2,1)S(1)}, u32[]{:S(2)}, u32[]{:S(2)}) collective-permute-start(bf16[256,256]{0,1:T(8,128)(2,1)S(1)} %fusion.61), channel_id=1, source_target_pairs={{0,4},{4,8},{8,12},{1,5},{5,9},{9,13},{2,6},{6,10},{10,14},{3,7},{... | collective-permute-start | bytes 393224 | tf_op jit(solution)/shard_map/ppermute | solution.py:16
  70.5 44.1 %collective-permute-start.5 = (bf16[256,256]{1,0:T(8,128)(2,1)S(1)}, bf16[256,256]{1,0:T(8,128)(2,1)S(1)}, u32[]{:S(2)}, u32[]{:S(2)}) collective-permute-start(bf16[256,256]{1,0:T(8,128)(2,1)S(1)} %convolution_convert_fusion.1), channel_id=1, source_target_pairs={{0,4},{4,8},{8,12},{1,5},{5,9},{9,13},{2,6},{6,10},{10,14},{3,7},{... | collective-permute-start | bytes 393224 | tf_op jit(solution)/shard_map/ppermute | solution.py:16
  76.1 38.5 %collective-permute-start = (bf16[256,256]{1,0:T(8,128)(2,1)S(1)}, bf16[256,256]{1,0:T(8,128)(2,1)S(1)}, u32[]{:S(2)}, u32[]{:S(2)}) collective-permute-start(bf16[256,256]{1,0:T(8,128)(2,1)S(1)} %convolution_convert_fusion.1), channel_id=1, source_target_pairs={{0,8},{4,12},{1,9},{5,13},{2,10},{6,14},{3,11},{7,15},{16,24},{20,... | collective-permute-start | bytes 393224 | tf_op jit(solution)/shard_map/ppermute | solution.py:16
  114.6 3.2 copy-start.11
  114.6 3.2 copy-start.14
  123.3 1.0 copy-start.9
  123.3 1.3 copy-start.10
  137.7 1.0 copy-start.8
  150.6 47.7 %all-gather.35.cloned.1.call-start = ((), (), s32[]{:S(2)}) async-start(), calls=%async_computation.8 | async-start | bytes 1310720 | tf_op jit(solution)/shard_map/all_gather | solution.py:118
  151.2 75.5 %all-gather.31.cloned.1.call-start = ((), (), s32[]{:S(2)}) async-start(), calls=%async_computation.6 | async-start | bytes 1310720 | tf_op jit(solution)/shard_map/all_gather | solution.py:123
  152.0 109.3 %all-gather.33.cloned.1.call-start = ((), (), s32[]{:S(2)}) async-start(), calls=%async_computation.7 | async-start | bytes 1310720 | tf_op jit(solution)/shard_map/all_gather | solution.py:113
  152.7 155.4 %all-gather.37.cloned.1.call-start = ((), (), s32[]{:S(2)}) async-start(), calls=%async_computation.9 | async-start | bytes 1310720 | tf_op jit(solution)/shard_map/all_gather | solution.py:148
  153.4 175.5 %all-gather.21.cloned.1.call-start = ((), (), s32[]{:S(2)}) async-start(), calls=%async_computation.1 | async-start | bytes 1310720 | tf_op jit(solution)/shard_map/all_gather | solution.py:153
  170.4 56.3 %copy-start.4 = (bf16[256,2048]{1,0:T(8,128)(2,1)S(1)}, bf16[256,2048]{1,0:T(8,128)(2,1)}, u32[]{:S(2)}) copy-start(bf16[256,2048]{1,0:T(8,128)(2,1)} %all-gather.19.cloned.1.call-done) | copy-start | bytes 3145732
  200.6 65.9 %collective-permute-start.7 = (bf16[256,256]{0,1:T(8,128)(2,1)S(1)}, bf16[256,256]{0,1:T(8,128)(2,1)S(1)}, u32[]{:S(2)}, u32[]{:S(2)}) collective-permute-start(bf16[256,256]{0,1:T(8,128)(2,1)S(1)} %fusion.59), channel_id=1, source_target_pairs={{0,8},{4,12},{1,9},{5,13},{2,10},{6,14},{3,11},{7,15},{16,24},{20,... | collective-permute-start | bytes 393224 | tf_op jit(solution)/shard_map/ppermute | solution.py:16
  204.4 63.4 %collective-permute-start.8 = (bf16[256,256]{0,1:T(8,128)(2,1)S(1)}, bf16[256,256]{0,1:T(8,128)(2,1)}, u32[]{:S(2)}, u32[]{:S(2)}) collective-permute-start(bf16[256,256]{0,1:T(8,128)(2,1)S(1)} %fusion.59), channel_id=1, source_target_pairs={{0,4},{4,8},{8,12},{1,5},{5,9},{9,13},{2,6},{6,10},{10,14},{3,7},{... | collective-permute-start | bytes 393224 | tf_op jit(solution)/shard_map/ppermute | solution.py:16
  229.1 56.4 %collective-permute-start.9 = (bf16[256,256]{1,0:T(8,128)(2,1)}, bf16[256,256]{1,0:T(8,128)(2,1)}, u32[]{:S(2)}, u32[]{:S(2)}) collective-permute-start(bf16[256,256]{1,0:T(8,128)(2,1)} %convolution_convert_fusion), channel_id=1, source_target_pairs={{0,4},{4,8},{8,12},{1,5},{5,9},{9,13},{2,6},{6,10},{10,14},{3,7},{... | collective-permute-start | bytes 393224 | tf_op jit(solution)/shard_map/ppermute | solution.py:16
  236.4 48.0 %collective-permute-start.6 = (bf16[256,256]{1,0:T(8,128)(2,1)}, bf16[256,256]{1,0:T(8,128)(2,1)}, u32[]{:S(2)}, u32[]{:S(2)}) collective-permute-start(bf16[256,256]{1,0:T(8,128)(2,1)} %convolution_convert_fusion), channel_id=1, source_target_pairs={{0,8},{4,12},{1,9},{5,13},{2,10},{6,14},{3,11},{7,15},{16,24},{20,... | collective-permute-start | bytes 393224 | tf_op jit(solution)/shard_map/ppermute | solution.py:16
  278.4 3.6 %copy-start.6 = (pred[4,64,576]{2,1,0:T(8,128)(4,1)S(1)}, pred[4,64,576]{2,1,0:T(8,128)(4,1)}, u32[]{:S(2)}) copy-start(pred[4,64,576]{2,1,0:T(8,128)(4,1)} %copy-done.5) | copy-start | bytes 442372
  284.4 5.1 %copy-start = (f32[4,4,64,576]{3,2,1,0:T(8,128)S(1)}, f32[4,4,64,576]{3,2,1,0:T(8,128)}, u32[]{:S(2)}) copy-start(f32[4,4,64,576]{3,2,1,0:T(8,128)} %get-tuple-element.66) | copy-start | bytes 7077892
  289.7 1.1 copy-start.1
  291.2 2.5 copy-start.2
  298.1 1.0 copy-start.7
Sparse Core Ops, SparseCore 0:
  8.9 30.7 all-gather.26
  41.2 27.4 all-gather.22
  70.3 30.6 all-gather.24
  102.4 31.1 all-gather.28
  150.8 18.0 all-gather.18
  170.3 27.9 all-gather.34
  199.9 26.7 all-gather.30
  228.2 32.9 all-gather.32
  262.8 30.7 all-gather.36
  310.8 18.0 all-gather.20
where the time goes:
time: 339 us; the launch traced here: 338 us
  waiting for transfers between devices  152 us (45%)
  matrix products  46.2 us (14%)
  local copies, waits for them, and re-layouts  45.6 us (13%)
  starting transfers between devices  44.3 us (13%)
  other arithmetic  19 us (6%)
  blocking collectives  17.1 us (5%)
  between operations  14.4 us (4%)
    ppermute x10, starting transfers between devices, shifted(): lax.ppermute(value, axis, [(source, source + steps) for source in range(i...  43.9 us
    all_gather x2, waiting for transfers between devices, on_device(): lax.all_gather(value_weight[layer], 'sp', axis=0, tiled=True)  39.8 us
    all_gather x2, waiting for transfers between devices, on_device(): lax.all_gather(query_weight[layer], 'sp', axis=0, tiled=True)  38.6 us
    all_gather x2, waiting for transfers between devices, on_device(): lax.all_gather(key_weight[layer], 'sp', axis=0, tiled=True)  37 us
    all_gather x2, waiting for transfers between devices, on_device(): x = lax.all_gather(new_cols, 'tp', axis=1, tiled=True)  33.5 us
    slice x20, local copies, waits for them, and re-layouts, attend(): value_blocks[earlier:earlier + count]  20.2 us
    dot_general x18, matrix products, attend(): jnp.einsum('nqhd,nkhd->nhqk', blocks, key_blocks[earlier:earlier + count]...  18.4 us
    all_gather x2, blocking collectives, on_device(): all_heads = lax.all_gather(attended, 'tp', axis=1, tiled=True)  17.1 us
  transfers between devices with their start and end apart: 20, of which 8 were waited for; matrix products, arithmetic and copies ran while one was open for 29% of the time, Pallas kernels for 0%

commit v1 on v0

--- a/solution.py
+++ b/solution.py
@@ -150,7 +150,14 @@
         )
         own_cols = lax.dynamic_slice_in_dim(widened, col_start, col_width, 1)
         new_cols = (own_cols + projected).astype(jnp.bfloat16)
-        x = lax.all_gather(new_cols, "tp", axis=1, tiled=True)
+        ring = [new_cols]
+        for hop in range(3):
+            ring.append(lax.ppermute(ring[-1], "tp", [(dev, (dev + 1) % 4) for dev in range(4)]))
+        x = jnp.roll(
+            jnp.concatenate(ring[::-1], axis=1),
+            (lax.axis_index("tp") + 1) * ring[0].shape[1],
+            axis=1,
+        )
     return x
 
 

time: 339 us -> 322 us (0.950)
  waiting for transfers between devices: 152 us -> 119 us
  other arithmetic: 19 us -> 25.6 us
  local copies, waits for them, and re-layouts: 45.6 us -> 49.8 us
  starting transfers between devices: 44.3 us -> 48.1 us
    ppermute x0 -> x6, waiting for transfers between devices: none -> 33.9 us  [on_device(): lax.ppermute(ring[-1], 'tp', [(dev, (dev + 1) % 4) for dev in range(4)])]
    all_gather x2 -> x0, waiting for transfers between devices: 33.5 us -> none  [on_device(): x = lax.all_gather(new_cols, 'tp', axis=1, tiled=True)]
    all_gather x2, waiting for transfers between devices: 37 us -> 7.7 us  [on_device(): lax.all_gather(key_weight[layer], 'sp', axis=0, tiled=True)]
    slice x20, local copies, waits for them, and re-layouts: 4 us -> 8.17 us  [attend(): key_blocks[earlier:earlier + count]]
    dot_general x18, matrix products: 10.9 us -> 14.7 us  [attend(): jnp.einsum('nhqk,nkhd->nqhd', part_weights, value_blocks[earlier:earlier...]
  transfers between devices with their start and end apart: 20 -> 24, of which waited for: 8 -> 11; matrix products, arithmetic and copies ran while one was open for 29% -> 37% of each run, Pallas kernels for 0% -> 0%
where the time goes in v1:
time: 322 us; the launch traced here: 321 us
  waiting for transfers between devices  119 us (37%)
  local copies, waits for them, and re-layouts  49.8 us (15%)
  matrix products  48.9 us (15%)
  starting transfers between devices  48.1 us (15%)
  other arithmetic  25.6 us (8%)
  blocking collectives  15.4 us (5%)
  between operations  14.4 us (4%)
    ppermute x10, starting transfers between devices, shifted(): lax.ppermute(value, axis, [(source, source + steps) for source in range(i...  47 us
    all_gather x2, waiting for transfers between devices, on_device(): lax.all_gather(query_weight[layer], 'sp', axis=0, tiled=True)  38.6 us
    all_gather x2, waiting for transfers between devices, on_device(): lax.all_gather(value_weight[layer], 'sp', axis=0, tiled=True)  37.2 us
    ppermute x6, waiting for transfers between devices, on_device(): lax.ppermute(ring[-1], 'tp', [(dev, (dev + 1) % 4) for dev in range(4)])  33.9 us
    slice x20, local copies, waits for them, and re-layouts, attend(): value_blocks[earlier:earlier + count]  19.7 us
    dot_general x18, matrix products, attend(): jnp.einsum('nqhd,nkhd->nhqk', blocks, key_blocks[earlier:earlier + count]...  18.7 us
    all_gather x2, blocking collectives, on_device(): all_heads = lax.all_gather(attended, 'tp', axis=1, tiled=True)  15.4 us
    dot_general x18, matrix products, attend(): jnp.einsum('nhqk,nkhd->nqhd', part_weights, value_blocks[earlier:earlier...  14.7 us
  transfers between devices with their start and end apart: 24, of which 11 were waited for; matrix products, arithmetic and copies ran while one was open for 37% of the time, Pallas kernels for 0%

profile of v1, /device:TPU:0, one launch (start us, length us, event | category | flops | bytes accessed | tf_op | source)
XLA Modules:
  0.0 320.9 jit_solution(4386245361868567081)
XLA Ops:
  6.5 2.0 fusion.273
  8.6 1.9 fusion.272
  13.6 6.0 %collective-permute-start.1 = (s32[256]{0:T(256)S(1)}, s32[256]{0:T(256)S(1)}, u32[]{:S(2)}, u32[]{:S(2)}) collective-permute-start(s32[256]{0:T(256)S(1)} %copy-done.27), channel_id=1, source_target_pairs={{0,8},{4,12},{1,9},{5,13},{2,10},{6,14},{3,11},{7,15},{16,24},{20,... | collective-permute-start | bytes 3080 | tf_op jit(solution)/shard_map/ppermute | solution.py:16
  19.6 3.5 %collective-permute-start.2 = (s32[256]{0:T(256)S(1)}, s32[256]{0:T(256)S(1)}, u32[]{:S(2)}, u32[]{:S(2)}) collective-permute-start(s32[256]{0:T(256)S(1)} %copy-done.27), channel_id=1, source_target_pairs={{0,4},{4,8},{8,12},{1,5},{5,9},{9,13},{2,6},{6,10},{10,14},{3,7},{... | collective-permute-start | bytes 3080 | tf_op jit(solution)/shard_map/ppermute | solution.py:16
  29.6 1.6 convert_element_type.52
  31.9 7.7 %all-gather.21.cloned.1.call-done = bf16[1,2048,256]{2,1,0:T(8,128)(2,1)} async-done(((bf16[1,512,256]{2,1,0:T(8,128)(2,1)}), bf16[1,2048,256]{2,1,0:T(8,128)(2,1)}) %all-gather.21.cloned.1.call-update) | async-done | bytes 1048592 | tf_op jit(solution)/shard_map/all_gather | solution.py:118
  39.6 1.9 bitcast_reduce_fusion.2
  41.6 3.8 %collective-permute-start.3 = (bf16[256,256]{0,1:T(8,128)(2,1)S(1)}, bf16[256,256]{0,1:T(8,128)(2,1)S(1)}, u32[]{:S(2)}, u32[]{:S(2)}) collective-permute-start(bf16[256,256]{0,1:T(8,128)(2,1)S(1)} %fusion.76), channel_id=1, source_target_pairs={{0,8},{4,12},{1,9},{5,13},{2,10},{6,14},{3,11},{7,15},{16,24},{20,... | collective-permute-start | bytes 393224 | tf_op jit(solution)/shard_map/ppermute | solution.py:16
  45.4 2.4 collective-permute-start.4
  48.1 20.3 %all-gather.17.cloned.1.call-done = bf16[1,2048,256]{2,1,0:T(8,128)(2,1)} async-done(((bf16[1,512,256]{2,1,0:T(8,128)(2,1)}), bf16[1,2048,256]{2,1,0:T(8,128)(2,1)}) %all-gather.17.cloned.1.call-update) | async-done | bytes 1048592 | tf_op jit(solution)/shard_map/all_gather | solution.py:123
  68.3 1.7 convolution_convert_fusion.1
  70.1 6.1 %collective-permute-start.5 = (bf16[256,256]{1,0:T(8,128)(2,1)S(1)}, bf16[256,256]{1,0:T(8,128)(2,1)S(1)}, u32[]{:S(2)}, u32[]{:S(2)}) collective-permute-start(bf16[256,256]{1,0:T(8,128)(2,1)S(1)} %convolution_convert_fusion.1), channel_id=1, source_target_pairs={{0,4},{4,8},{8,12},{1,5},{5,9},{9,13},{2,6},{6,10},{10,14},{3,7},{... | collective-permute-start | bytes 393224 | tf_op jit(solution)/shard_map/ppermute | solution.py:16
  76.2 4.3 %collective-permute-start = (bf16[256,256]{1,0:T(8,128)(2,1)S(1)}, bf16[256,256]{1,0:T(8,128)(2,1)S(1)}, u32[]{:S(2)}, u32[]{:S(2)}) collective-permute-start(bf16[256,256]{1,0:T(8,128)(2,1)S(1)} %convolution_convert_fusion.1), channel_id=1, source_target_pairs={{0,8},{4,12},{1,9},{5,13},{2,10},{6,14},{3,11},{7,15},{16,24},{20,... | collective-permute-start | bytes 393224 | tf_op jit(solution)/shard_map/ppermute | solution.py:16
  81.4 19.7 %all-gather.19.cloned.1.call-done = bf16[1,2048,256]{2,1,0:T(8,128)(2,1)} async-done(((bf16[1,512,256]{2,1,0:T(8,128)(2,1)}), bf16[1,2048,256]{2,1,0:T(8,128)(2,1)}) %all-gather.19.cloned.1.call-update) | async-done | bytes 1048592 | tf_op jit(solution)/shard_map/all_gather | solution.py:113
  101.1 1.9 bitcast_reduce_fusion.3
  118.0 3.6 %concatenate.101 = f32[4,4,64,576]{3,2,1,0:T(8,128)S(1)} concatenate(f32[4,4,64,64]{3,2,1,0:T(8,128)} %fusion.129, f32[4,4,64,64]{3,2,1,0:T(8,128)} %fusion.127, f32[4,4,64,64]{3,2,1,0:T(8,128)} %fusion.125, f32[4,4,64,64]{3,2,1,0:T(8,128)} %fusion.123, f32[4,4,64,64]{3,2,1,0:T(8,128)} %fusion.121, f32[4,4,64,64]{3,2,1,0:T(8,128)} %fusion.119, f32[4,4,64,64]{3,2,1,0:T(8,128)} %fusion.117, ...), dimensions={3} | concatenate | bytes 4718592 | tf_op jit(solution)/shard_map/concatenate | solution.py:54
  131.7 8.7 %all_gather.33 = bf16[256,1024]{1,0:T(8,128)(2,1)S(1)} all-gather(bf16[256,256]{1,0:T(8,128)(2,1)S(1)} %reshape.224), channel_id=1, replica_groups=mesh['grp'=2,'sp'=4,'tp'=4] {'tp'}, dimensions={1}, use_global_device_ids=true | all-gather | bytes 655360 | tf_op jit(solution)/shard_map/all_gather | solution.py:145
  140.4 1.8 fusion.16
  142.7 5.4 %collective-permute-done.6 = bf16[256,512]{1,0:T(8,128)(2,1)S(1)} collective-permute-done((bf16[256,512]{1,0:T(8,128)(2,1)S(1)}, bf16[256,512]{1,0:T(8,128)(2,1)S(1)}, u32[]{:S(2)}, u32[]{:S(2)}) %collective-permute-start.6) | collective-permute-done | bytes 262176 | tf_op jit(solution)/shard_map/ppermute | solution.py:155
  148.1 5.8 %collective-permute-done.7 = bf16[256,512]{1,0:T(8,128)(2,1)S(1)} collective-permute-done((bf16[256,512]{1,0:T(8,128)(2,1)S(1)}, bf16[256,512]{1,0:T(8,128)(2,1)S(1)}, u32[]{:S(2)}, u32[]{:S(2)}) %collective-permute-start.7) | collective-permute-done | bytes 262176 | tf_op jit(solution)/shard_map/ppermute | solution.py:155
  154.1 5.7 %collective-permute-done.8 = bf16[256,512]{1,0:T(8,128)(2,1)S(1)} collective-permute-done((bf16[256,512]{1,0:T(8,128)(2,1)S(1)}, bf16[256,512]{1,0:T(8,128)(2,1)S(1)}, u32[]{:S(2)}, u32[]{:S(2)}) %collective-permute-start.8) | collective-permute-done | bytes 262176 | tf_op jit(solution)/shard_map/ppermute | solution.py:155
  159.7 3.0 multiply_reduce_fusion
  163.0 1.8 bitcast_reduce_fusion
  164.9 5.8 %collective-permute-start.10 = (bf16[256,256]{0,1:T(8,128)(2,1)S(1)}, bf16[256,256]{0,1:T(8,128)(2,1)}, u32[]{:S(2)}, u32[]{:S(2)}) collective-permute-start(bf16[256,256]{0,1:T(8,128)(2,1)S(1)} %fusion.74), channel_id=1, source_target_pairs={{0,8},{4,12},{1,9},{5,13},{2,10},{6,14},{3,11},{7,15},{16,24},{20,... | collective-permute-start | bytes 393224 | tf_op jit(solution)/shard_map/ppermute | solution.py:16
  170.7 3.9 %collective-permute-start.11 = (bf16[256,256]{0,1:T(8,128)(2,1)S(1)}, bf16[256,256]{0,1:T(8,128)(2,1)}, u32[]{:S(2)}, u32[]{:S(2)}) collective-permute-start(bf16[256,256]{0,1:T(8,128)(2,1)S(1)} %fusion.74), channel_id=1, source_target_pairs={{0,4},{4,8},{8,12},{1,5},{5,9},{9,13},{2,6},{6,10},{10,14},{3,7},{... | collective-permute-start | bytes 393224 | tf_op jit(solution)/shard_map/ppermute | solution.py:16
  175.5 16.9 %all-gather.25.cloned.1.call-done = bf16[1,2048,256]{2,1,0:T(8,128)(2,1)} async-done(((bf16[1,512,256]{2,1,0:T(8,128)(2,1)}), bf16[1,2048,256]{2,1,0:T(8,128)(2,1)}) %all-gather.25.cloned.1.call-update) | async-done | bytes 1048592 | tf_op jit(solution)/shard_map/all_gather | solution.py:123
  192.4 2.3 convolution_convert_fusion
  194.7 6.1 %collective-permute-start.12 = (bf16[256,256]{1,0:T(8,128)(2,1)}, bf16[256,256]{1,0:T(8,128)(2,1)}, u32[]{:S(2)}, u32[]{:S(2)}) collective-permute-start(bf16[256,256]{1,0:T(8,128)(2,1)} %convolution_convert_fusion), channel_id=1, source_target_pairs={{0,4},{4,8},{8,12},{1,5},{5,9},{9,13},{2,6},{6,10},{10,14},{3,7},{... | collective-permute-start | bytes 393224 | tf_op jit(solution)/shard_map/ppermute | solution.py:16
  200.8 5.1 %collective-permute-start.9 = (bf16[256,256]{1,0:T(8,128)(2,1)}, bf16[256,256]{1,0:T(8,128)(2,1)}, u32[]{:S(2)}, u32[]{:S(2)}) collective-permute-start(bf16[256,256]{1,0:T(8,128)(2,1)} %convolution_convert_fusion), channel_id=1, source_target_pairs={{0,8},{4,12},{1,9},{5,13},{2,10},{6,14},{3,11},{7,15},{16,24},{20,... | collective-permute-start | bytes 393224 | tf_op jit(solution)/shard_map/ppermute | solution.py:16
  205.9 1.8 slice.729
  207.7 18.9 %all-gather.27.cloned.1.call-done = bf16[1,2048,256]{2,1,0:T(8,128)(2,1)} async-done(((bf16[1,512,256]{2,1,0:T(8,128)(2,1)}), bf16[1,2048,256]{2,1,0:T(8,128)(2,1)}) %all-gather.27.cloned.1.call-update) | async-done | bytes 1048592 | tf_op jit(solution)/shard_map/all_gather | solution.py:113
  226.6 2.5 bitcast_reduce_fusion.1
  235.0 1.9 pad_maximum_fusion.1
  248.8 4.7 %concatenate.108 = f32[4,4,64,576]{3,2,1,0:T(8,128)} concatenate(f32[4,4,64,64]{3,2,1,0:T(8,128)} %fusion.102, f32[4,4,64,64]{3,2,1,0:T(8,128)} %fusion.100, f32[4,4,64,64]{3,2,1,0:T(8,128)} %fusion.98, f32[4,4,64,64]{3,2,1,0:T(8,128)} %fusion.96, f32[4,4,64,64]{3,2,1,0:T(8,128)} %fusion.94, f32[4,4,64,64]{3,2,1,0:T(8,128)} %fusion.92, f32[4,4,64,64]{3,2,1,0:T(8,128)} %fusion.90, ...), dimensions={3} | concatenate | bytes 4718592 | tf_op jit(solution)/shard_map/concatenate | solution.py:54
  253.6 4.1 %fusion.283 = (f32[4,4,64]{2,1,0:T(4,128)S(1)}, f32[4,4,64,576]{3,2,1,0:T(8,128)}) fusion(f32[4,4,64,576]{3,2,1,0:T(8,128)} %concatenate.108, f32[4,64,576]{2,1,0:T(8,128)S(1)} %copy-done.1, pred[4,64,576]{2,1,0:T(8,128)(4,1)S(1)} %copy-done.4), kind=kOutput, calls=%fused_computation.567 | output fusion | flops 2949695 | bytes 5459968 | tf_op jit(solution)/shard_map/sub | solution.py:70
  258.6 1.8 pad_maximum_fusion
  263.7 2.0 divide_convert_fusion
  268.0 1.8 slice.688
  269.8 2.5 fusion.13
  273.4 1.8 slice.716
  275.2 1.8 slice.724
  277.8 1.8 slice.718
  286.0 6.7 %all_gather.38 = bf16[256,1024]{1,0:T(8,128)(2,1)S(1)} all-gather(bf16[256,256]{1,0:T(8,128)(2,1)S(1)} %reshape.226), channel_id=1, replica_groups=mesh['grp'=2,'sp'=4,'tp'=4] {'tp'}, dimensions={1}, use_global_device_ids=true | all-gather | bytes 655360 | tf_op jit(solution)/shard_map/all_gather | solution.py:145
  292.7 1.7 fusion.17
  294.8 5.4 %collective-permute-done.13 = bf16[256,512]{1,0:T(8,128)(2,1)S(1)} collective-permute-done((bf16[256,512]{1,0:T(8,128)(2,1)S(1)}, bf16[256,512]{1,0:T(8,128)(2,1)S(1)}, u32[]{:S(2)}, u32[]{:S(2)}) %collective-permute-start.13) | collective-permute-done | bytes 262176 | tf_op jit(solution)/shard_map/ppermute | solution.py:155
  300.2 5.8 %collective-permute-done.14 = bf16[256,512]{1,0:T(8,128)(2,1)S(1)} collective-permute-done((bf16[256,512]{1,0:T(8,128)(2,1)S(1)}, bf16[256,512]{1,0:T(8,128)(2,1)S(1)}, u32[]{:S(2)}, u32[]{:S(2)}) %collective-permute-start.14) | collective-permute-done | bytes 262176 | tf_op jit(solution)/shard_map/ppermute | solution.py:155
  306.0 5.8 %collective-permute-done.15 = bf16[256,512]{1,0:T(8,128)(2,1)S(1)} collective-permute-done((bf16[256,512]{1,0:T(8,128)(2,1)S(1)}, bf16[256,512]{1,0:T(8,128)(2,1)S(1)}, u32[]{:S(2)}, u32[]{:S(2)}) %collective-permute-start.15) | collective-permute-done | bytes 262176 | tf_op jit(solution)/shard_map/ppermute | solution.py:155
  311.8 2.3 fusion.25
  (285 shorter events, 70.9 us)
Async XLA Ops:
  6.5 4.0 %copy-start.17 = (bf16[2,512,256]{2,1,0:T(8,128)(2,1)S(1)}, bf16[2,512,256]{2,1,0:T(8,128)(2,1)}, u32[]{:S(2)}) copy-start(bf16[2,512,256]{2,1,0:T(8,128)(2,1)} %param.15) | copy-start | bytes 1572868
  6.5 5.0 %copy-start.18 = (bf16[2,256,512]{2,1,0:T(8,128)(2,1)S(1)}, bf16[2,256,512]{2,1,0:T(8,128)(2,1)}, u32[]{:S(2)}) copy-start(bf16[2,256,512]{2,1,0:T(8,128)(2,1)} %param.18) | copy-start | bytes 1572868
  6.5 33.0 %all-gather.21.cloned.1.call-start = ((), (), s32[]{:S(2)}) async-start(), calls=%async_computation.2 | async-start | bytes 1310720 | tf_op jit(solution)/shard_map/all_gather | solution.py:118
  8.5 5.1 %copy-start.27 = (s32[256]{0:T(256)S(1)}, s32[256]{0:T(256)}, u32[]{:S(2)}) copy-start(s32[256]{0:T(256)} %param.13) | copy-start | bytes 3076
  8.5 59.8 %all-gather.17.cloned.1.call-start = ((), (), s32[]{:S(2)}) async-start(), calls=%async_computation | async-start | bytes 1310720 | tf_op jit(solution)/shard_map/all_gather | solution.py:123
  10.5 12.7 %copy-start.26 = (f32[4,513]{1,0:T(4,128)S(1)}, f32[4,513]{1,0:T(4,128)}, u32[]{:S(2)}) copy-start(f32[4,513]{1,0:T(4,128)} %param.21) | copy-start | bytes 24628
  10.5 12.9 %copy-start.25 = (f32[2,2048]{1,0:T(2,128)S(1)}, f32[2,2048]{1,0:T(2,128)}, u32[]{:S(2)}) copy-start(f32[2,2048]{1,0:T(2,128)} %param.14) | copy-start | bytes 49156
  10.5 13.0 %copy-start.2 = (bf16[256,2048]{1,0:T(8,128)(2,1)S(1)}, bf16[256,2048]{1,0:T(8,128)(2,1)}, u32[]{:S(2)}) copy-start(bf16[256,2048]{1,0:T(8,128)(2,1)} %param.12) | copy-start | bytes 3145732
  10.5 13.2 %copy-start.28 = (f32[2,64]{1,0:T(2,128)S(1)}, f32[2,64]{1,0:T(2,128)}, u32[]{:S(2)}) copy-start(f32[2,64]{1,0:T(2,128)} %param.19) | copy-start | bytes 1540
  10.5 13.2 %copy-start.29 = (f32[2,64]{1,0:T(2,128)S(1)}, f32[2,64]{1,0:T(2,128)}, u32[]{:S(2)}) copy-start(f32[2,64]{1,0:T(2,128)} %param.20) | copy-start | bytes 1540
  10.5 90.5 %all-gather.19.cloned.1.call-start = ((), (), s32[]{:S(2)}) async-start(), calls=%async_computation.1 | async-start | bytes 1310720 | tf_op jit(solution)/shard_map/all_gather | solution.py:113
  11.5 129.0 %all-gather.23.cloned.1.call-start = ((), (), s32[]{:S(2)}) async-start(), calls=%async_computation.3 | async-start | bytes 1310720 | tf_op jit(solution)/shard_map/all_gather | solution.py:148
  12.4 150.6 %all-gather.29.cloned.1.call-start = ((), (), s32[]{:S(2)}) async-start(), calls=%async_computation.6 | async-start | bytes 1310720 | tf_op jit(solution)/shard_map/all_gather | solution.py:118
  13.0 179.4 %all-gather.25.cloned.1.call-start = ((), (), s32[]{:S(2)}) async-start(), calls=%async_computation.4 | async-start | bytes 1310720 | tf_op jit(solution)/shard_map/all_gather | solution.py:123
  13.6 213.0 %all-gather.27.cloned.1.call-start = ((), (), s32[]{:S(2)}) async-start(), calls=%async_computation.5 | async-start | bytes 1310720 | tf_op jit(solution)/shard_map/all_gather | solution.py:113
  13.6 17.8 %collective-permute-start.1 = (s32[256]{0:T(256)S(1)}, s32[256]{0:T(256)S(1)}, u32[]{:S(2)}, u32[]{:S(2)}) collective-permute-start(s32[256]{0:T(256)S(1)} %copy-done.27), channel_id=1, source_target_pairs={{0,8},{4,12},{1,9},{5,13},{2,10},{6,14},{3,11},{7,15},{16,24},{20,... | collective-permute-start | bytes 3080 | tf_op jit(solution)/shard_map/ppermute | solution.py:16
  19.6 11.9 %collective-permute-start.2 = (s32[256]{0:T(256)S(1)}, s32[256]{0:T(256)S(1)}, u32[]{:S(2)}, u32[]{:S(2)}) collective-permute-start(s32[256]{0:T(256)S(1)} %copy-done.27), channel_id=1, source_target_pairs={{0,4},{4,8},{8,12},{1,5},{5,9},{9,13},{2,6},{6,10},{10,14},{3,7},{... | collective-permute-start | bytes 3080 | tf_op jit(solution)/shard_map/ppermute | solution.py:16
  23.1 269.6 %all-gather.31.cloned.1.call-start = ((), (), s32[]{:S(2)}) async-start(), calls=%async_computation.7 | async-start | bytes 1310720 | tf_op jit(solution)/shard_map/all_gather | solution.py:148
  31.4 90.2 %copy-start = (f32[4,64,576]{2,1,0:T(8,128)}, f32[4,64,576]{2,1,0:T(8,128)S(1)}, u32[]{:S(2)}) copy-start(f32[4,64,576]{2,1,0:T(8,128)S(1)} %copy.61) | copy-start | bytes 1769476
  31.9 89.7 %copy-start.3 = (pred[4,64,576]{2,1,0:T(8,128)(4,1)}, pred[4,64,576]{2,1,0:T(8,128)(4,1)S(1)}, u32[]{:S(2)}) copy-start(pred[4,64,576]{2,1,0:T(8,128)(4,1)S(1)} %compare_and_fusion) | copy-start | bytes 442372
  41.6 63.1 %collective-permute-start.3 = (bf16[256,256]{0,1:T(8,128)(2,1)S(1)}, bf16[256,256]{0,1:T(8,128)(2,1)S(1)}, u32[]{:S(2)}, u32[]{:S(2)}) collective-permute-start(bf16[256,256]{0,1:T(8,128)(2,1)S(1)} %fusion.76), channel_id=1, source_target_pairs={{0,8},{4,12},{1,9},{5,13},{2,10},{6,14},{3,11},{7,15},{16,24},{20,... | collective-permute-start | bytes 393224 | tf_op jit(solution)/shard_map/ppermute | solution.py:16
  45.4 60.5 %collective-permute-start.4 = (bf16[256,256]{0,1:T(8,128)(2,1)S(1)}, bf16[256,256]{0,1:T(8,128)(2,1)S(1)}, u32[]{:S(2)}, u32[]{:S(2)}) collective-permute-start(bf16[256,256]{0,1:T(8,128)(2,1)S(1)} %fusion.76), channel_id=1, source_target_pairs={{0,4},{4,8},{8,12},{1,5},{5,9},{9,13},{2,6},{6,10},{10,14},{3,7},{... | collective-permute-start | bytes 393224 | tf_op jit(solution)/shard_map/ppermute | solution.py:16
  70.1 44.7 %collective-permute-start.5 = (bf16[256,256]{1,0:T(8,128)(2,1)S(1)}, bf16[256,256]{1,0:T(8,128)(2,1)S(1)}, u32[]{:S(2)}, u32[]{:S(2)}) collective-permute-start(bf16[256,256]{1,0:T(8,128)(2,1)S(1)} %convolution_convert_fusion.1), channel_id=1, source_target_pairs={{0,4},{4,8},{8,12},{1,5},{5,9},{9,13},{2,6},{6,10},{10,14},{3,7},{... | collective-permute-start | bytes 393224 | tf_op jit(solution)/shard_map/ppermute | solution.py:16
  76.2 38.6 %collective-permute-start = (bf16[256,256]{1,0:T(8,128)(2,1)S(1)}, bf16[256,256]{1,0:T(8,128)(2,1)S(1)}, u32[]{:S(2)}, u32[]{:S(2)}) collective-permute-start(bf16[256,256]{1,0:T(8,128)(2,1)S(1)} %convolution_convert_fusion.1), channel_id=1, source_target_pairs={{0,8},{4,12},{1,9},{5,13},{2,10},{6,14},{3,11},{7,15},{16,24},{20,... | collective-permute-start | bytes 393224 | tf_op jit(solution)/shard_map/ppermute | solution.py:16
  114.7 2.4 copy-start.15
  114.7 2.4 copy-start.19
  122.6 1.6 copy-start.23
  123.6 2.1 copy-start.21
  123.9 3.0 copy-start.16
  127.8 1.7 copy-start.20
  142.3 5.8 %collective-permute-start.6 = (bf16[256,512]{1,0:T(8,128)(2,1)S(1)}, bf16[256,512]{1,0:T(8,128)(2,1)S(1)}, u32[]{:S(2)}, u32[]{:S(2)}) collective-permute-start(bf16[256,512]{1,0:T(8,128)(2,1)S(1)} %fusion.16), channel_id=1, source_target_pairs={{0,1},{1,2},{2,3},{3,0},{4,5},{5,6},{6,7},{7,4},{8,9},{9,10},{10,1... | collective-permute-start | bytes 786440 | tf_op jit(solution)/shard_map/ppermute | solution.py:155
  148.1 5.8 %collective-permute-start.7 = (bf16[256,512]{1,0:T(8,128)(2,1)S(1)}, bf16[256,512]{1,0:T(8,128)(2,1)S(1)}, u32[]{:S(2)}, u32[]{:S(2)}) collective-permute-start(bf16[256,512]{1,0:T(8,128)(2,1)S(1)} %collective-permute-done.6), channel_id=1, source_target_pairs={{0,1},{1,2},{2,3},{3,0},{4,5},{5,6},{6,7},{7,4},{8,9},{9,10},{10,1... | collective-permute-start | bytes 786440 | tf_op jit(solution)/shard_map/ppermute | solution.py:155
  153.9 5.8 %collective-permute-start.8 = (bf16[256,512]{1,0:T(8,128)(2,1)S(1)}, bf16[256,512]{1,0:T(8,128)(2,1)S(1)}, u32[]{:S(2)}, u32[]{:S(2)}) collective-permute-start(bf16[256,512]{1,0:T(8,128)(2,1)S(1)} %collective-permute-done.7), channel_id=1, source_target_pairs={{0,1},{1,2},{2,3},{3,0},{4,5},{5,6},{6,7},{7,4},{8,9},{9,10},{10,1... | collective-permute-start | bytes 786440 | tf_op jit(solution)/shard_map/ppermute | solution.py:155
  164.9 67.0 %collective-permute-start.10 = (bf16[256,256]{0,1:T(8,128)(2,1)S(1)}, bf16[256,256]{0,1:T(8,128)(2,1)}, u32[]{:S(2)}, u32[]{:S(2)}) collective-permute-start(bf16[256,256]{0,1:T(8,128)(2,1)S(1)} %fusion.74), channel_id=1, source_target_pairs={{0,8},{4,12},{1,9},{5,13},{2,10},{6,14},{3,11},{7,15},{16,24},{20,... | collective-permute-start | bytes 393224 | tf_op jit(solution)/shard_map/ppermute | solution.py:16
  170.7 64.2 %collective-permute-start.11 = (bf16[256,256]{0,1:T(8,128)(2,1)S(1)}, bf16[256,256]{0,1:T(8,128)(2,1)}, u32[]{:S(2)}, u32[]{:S(2)}) collective-permute-start(bf16[256,256]{0,1:T(8,128)(2,1)S(1)} %fusion.74), channel_id=1, source_target_pairs={{0,4},{4,8},{8,12},{1,5},{5,9},{9,13},{2,6},{6,10},{10,14},{3,7},{... | collective-permute-start | bytes 393224 | tf_op jit(solution)/shard_map/ppermute | solution.py:16
  194.7 63.9 %collective-permute-start.12 = (bf16[256,256]{1,0:T(8,128)(2,1)}, bf16[256,256]{1,0:T(8,128)(2,1)}, u32[]{:S(2)}, u32[]{:S(2)}) collective-permute-start(bf16[256,256]{1,0:T(8,128)(2,1)} %convolution_convert_fusion), channel_id=1, source_target_pairs={{0,4},{4,8},{8,12},{1,5},{5,9},{9,13},{2,6},{6,10},{10,14},{3,7},{... | collective-permute-start | bytes 393224 | tf_op jit(solution)/shard_map/ppermute | solution.py:16
  200.8 56.9 %collective-permute-start.9 = (bf16[256,256]{1,0:T(8,128)(2,1)}, bf16[256,256]{1,0:T(8,128)(2,1)}, u32[]{:S(2)}, u32[]{:S(2)}) collective-permute-start(bf16[256,256]{1,0:T(8,128)(2,1)} %convolution_convert_fusion), channel_id=1, source_target_pairs={{0,8},{4,12},{1,9},{5,13},{2,10},{6,14},{3,11},{7,15},{16,24},{20,... | collective-permute-start | bytes 393224 | tf_op jit(solution)/shard_map/ppermute | solution.py:16
  238.9 6.4 %copy-start.24 = (bf16[256,256]{0,1:T(8,128)(2,1)S(1)}, bf16[256,256]{0,1:T(8,128)(2,1)}, u32[]{:S(2)}) copy-start(bf16[256,256]{0,1:T(8,128)(2,1)} %get-tuple-element.23) | copy-start | bytes 393220
  248.8 4.7 %copy-start.1 = (f32[4,64,576]{2,1,0:T(8,128)S(1)}, f32[4,64,576]{2,1,0:T(8,128)}, u32[]{:S(2)}) copy-start(f32[4,64,576]{2,1,0:T(8,128)} %copy-done) | copy-start | bytes 1769476
  248.8 4.7 %copy-start.4 = (pred[4,64,576]{2,1,0:T(8,128)(4,1)S(1)}, pred[4,64,576]{2,1,0:T(8,128)(4,1)}, u32[]{:S(2)}) copy-start(pred[4,64,576]{2,1,0:T(8,128)(4,1)} %copy-done.3) | copy-start | bytes 442372
  263.7 2.0 copy-start.13
  263.7 3.2 copy-start.14
  269.8 2.5 copy-start.8
  279.6 3.0 copy-start.10
  281.2 1.8 copy-start.11
  294.4 5.8 %collective-permute-start.13 = (bf16[256,512]{1,0:T(8,128)(2,1)S(1)}, bf16[256,512]{1,0:T(8,128)(2,1)S(1)}, u32[]{:S(2)}, u32[]{:S(2)}) collective-permute-start(bf16[256,512]{1,0:T(8,128)(2,1)S(1)} %fusion.17), channel_id=1, source_target_pairs={{0,1},{1,2},{2,3},{3,0},{4,5},{5,6},{6,7},{7,4},{8,9},{9,10},{10,1... | collective-permute-start | bytes 786440 | tf_op jit(solution)/shard_map/ppermute | solution.py:155
  300.2 5.8 %collective-permute-start.14 = (bf16[256,512]{1,0:T(8,128)(2,1)S(1)}, bf16[256,512]{1,0:T(8,128)(2,1)S(1)}, u32[]{:S(2)}, u32[]{:S(2)}) collective-permute-start(bf16[256,512]{1,0:T(8,128)(2,1)S(1)} %collective-permute-done.13), channel_id=1, source_target_pairs={{0,1},{1,2},{2,3},{3,0},{4,5},{5,6},{6,7},{7,4},{8,9},{9,10},{10,1... | collective-permute-start | bytes 786440 | tf_op jit(solution)/shard_map/ppermute | solution.py:155
  306.0 5.8 %collective-permute-start.15 = (bf16[256,512]{1,0:T(8,128)(2,1)S(1)}, bf16[256,512]{1,0:T(8,128)(2,1)S(1)}, u32[]{:S(2)}, u32[]{:S(2)}) collective-permute-start(bf16[256,512]{1,0:T(8,128)(2,1)S(1)} %collective-permute-done.14), channel_id=1, source_target_pairs={{0,1},{1,2},{2,3},{3,0},{4,5},{5,6},{6,7},{7,4},{8,9},{9,10},{10,1... | collective-permute-start | bytes 786440 | tf_op jit(solution)/shard_map/ppermute | solution.py:155
  (6 other events, 6.8 us)
Sparse Core Ops, SparseCore 0:
  8.9 30.6 all-gather.20
  41.1 27.1 all-gather.16
  69.9 31.0 all-gather.18
  102.5 31.1 all-gather.22
  135.1 27.3 all-gather.28
  163.9 28.4 all-gather.24
  194.0 32.5 all-gather.26
  228.1 29.4 all-gather.30
